TPU v7x, 256 devices: a whole 4x4x8 slice. The times are simulated.
256 devices in a mesh: sp: 16 (over y, x), tp: 16 (over z, core).
Axes of the slice: x: 4, y: 4, z: 8, core: 2. Of those that a mesh axis runs over, the one named last changes fastest.
Arguments:
- tokens: bfloat16 [8192, 2048], P(('sp', 'tp')), may hold values from -6 to 6
- query_vectors: bfloat16 [8192, 2048], P('sp', 'tp'), may hold values from -8 to 8
- key_vectors: bfloat16 [8192, 2048], P('sp', 'tp'), may hold values from -8 to 8
- value_vectors: bfloat16 [8192, 2048], P('sp', 'tp'), may hold values from -24 to 24
- cum_gate: float32 [8192, 32], P('sp', 'tp'), may hold values from -1028 to 0, as said below
- out_weight: bfloat16 [2048, 2048], P('tp'), may hold values from -0.125 to 0.125
- norm_gain: float32 [2048], replicated, may hold values from 0.1 to 1.9
- gate_weight: bfloat16 [16, 2048, 7168], P('sp', None, 'tp'), may hold values from -0.125 to 0.125
- up_weight: bfloat16 [16, 2048, 7168], P('sp', None, 'tp'), may hold values from -0.125 to 0.125
- down_weight: bfloat16 [16, 7168, 2048], P('sp', 'tp'), may hold values from -0.0625 to 0.0625
- expert_ids: int32 [8192, 2], P(('sp', 'tp')), may hold values from 0 to 15, all different within a row; in each aligned block of 32 rows (0 to 31, 32 to 63, ...) at most 6 rows name the same one
- route_weights: float32 [8192, 2], P(('sp', 'tp')), may hold values from 0.2 to 1
Outputs:
- layer_output: bfloat16 [8192, 2048], P(('sp', 'tp'))
Inputs may be any that keep to these rules, and one draw needn't show every extreme that they name: `cum_gate`: along the positions each head's values never rise. `expert_ids`: within the rows of one device no expert is named by more than 6 rows, and in some devices' rows one expert is named by exactly 6; a row names 2 different experts.
All inputs are finite; a program needn't handle non-finite values.
Results may differ from a plain program's by a relative error of at most 0.014.
Values may be sent and summed in bfloat16 or wider, within the bound.
A program may use at most 128 MiB of HBM per device.

v0:
```python
import math
import jax
import jax.numpy as jnp
from jax import lax
from jax.sharding import PartitionSpec as P

NEG_LARGE = -1e30


def copy_for_each(shard, axis):
    peers = lax.axis_size(axis)
    return lax.all_to_all(
        jnp.broadcast_to(shard[None], (peers, *shard.shape)), axis, 0, 0, tiled=True
    )


def in_order(parts, dim):
    parts = jnp.moveaxis(parts, 0, dim)
    dims = parts.shape
    return parts.reshape(*dims[:dim], dims[dim] * dims[dim + 1], *dims[dim + 2 :])


def collect(shard, axis, dim):
    parts = copy_for_each(shard, axis)
    return in_order(parts, dim)


def sent_together(arrays, axis, dim, along):
    widths = [a.shape[along] for a in arrays]
    both = jnp.concatenate(arrays, axis=along)
    filled = lax.all_gather(both, axis, axis=dim, tiled=True)
    return tuple(jnp.split(filled, [sum(widths[:k]) for k in range(1, len(widths))], axis=along))


def shards(
    tokens,
    query_vectors,
    key_vectors,
    value_vectors,
    cum_gate,
    out_weight,
    norm_gain,
    gate_weight,
    up_weight,
    down_weight,
    expert_ids,
    route_weights,
):
    sp_count = lax.axis_size("sp")
    seg_rows = query_vectors.shape[0]
    heads_here = cum_gate.shape[1]
    head_width = query_vectors.shape[1] // heads_here
    score_scale = head_width ** (-0.5)
    offset = lax.axis_index("sp") * seg_rows
    last_query = offset + seg_rows - 1
    query_pos = offset + jnp.arange(seg_rows, dtype=jnp.int32)
    query_heads = query_vectors.reshape(seg_rows, heads_here, head_width)
    query_gate = cum_gate.T
    gate_rows = collect(cum_gate, "sp", 0)

    def attend_block(carried, key_block, value_block, block_start):
        running_peak, running_total, accumulated = carried
        row_count = key_block.shape[0]
        key_heads = key_block.reshape(row_count, heads_here, head_width)
        value_heads = value_block.reshape(row_count, heads_here, head_width)
        key_gate = lax.dynamic_slice_in_dim(gate_rows, block_start, row_count, 0).T
        scores = (
            jnp.einsum("qhd,khd->hqk", query_heads, key_heads, preferred_element_type=jnp.float32)
            * score_scale
        )
        scores = scores + query_gate[:, :, None] - key_gate[:, None, :]
        key_pos = block_start + jnp.arange(row_count, dtype=jnp.int32)
        visible = (key_pos[None, :] <= query_pos[:, None])[None]
        scores = jnp.where(visible, scores, NEG_LARGE)
        new_peak = jnp.maximum(running_peak, jnp.max(scores, axis=2))
        exponent = jnp.where(visible, jnp.exp(scores - new_peak[:, :, None]), 0.0)
        rescale = jnp.exp(running_peak - new_peak)
        running_total = running_total * rescale + jnp.sum(exponent, axis=2)
        weighted = jnp.einsum(
            "hqk,khd->hqd",
            exponent.astype(jnp.bfloat16),
            value_heads,
            preferred_element_type=jnp.float32,
        )
        accumulated = accumulated * rescale[:, :, None] + weighted
        return (new_peak, running_total, accumulated)

    start_state = (
        jnp.full((heads_here, seg_rows), NEG_LARGE, jnp.float32),
        jnp.zeros((heads_here, seg_rows), jnp.float32),
        jnp.zeros((heads_here, seg_rows, head_width), jnp.float32),
    )
    carried = start_state
    key_piece, value_piece = sent_together((key_vectors, value_vectors), "sp", 0, 1)
    row_count = key_piece.shape[0]
    block_rows = math.gcd(row_count, 1024)
    block_count = row_count // block_rows
    key_stack = key_piece.reshape(block_count, block_rows, key_piece.shape[1])
    value_stack = value_piece.reshape(block_count, block_rows, value_piece.shape[1])

    def step_block(state, inputs):
        key_block, value_block, block_index = inputs
        block_start = block_index * block_rows

        def take_block(inner):
            return attend_block(inner, key_block, value_block, block_start)

        def skip_block(inner):
            return inner

        return (lax.cond(block_start <= last_query, take_block, skip_block, state), None)

    carried, _ = lax.scan(
        step_block, carried, (key_stack, value_stack, jnp.arange(block_count, dtype=jnp.int32))
    )
    final_peak, final_total, accumulated = carried
    attended = (accumulated / final_total[:, :, None]).astype(jnp.bfloat16)
    attended = attended.transpose(1, 0, 2).reshape(seg_rows, heads_here * head_width)
    tok_dev = tokens.shape[0]
    model_width = tokens.shape[1]
    token_rows = lax.all_to_all(attended, "tp", split_axis=0, concat_axis=1, tiled=True)
    projected = jnp.dot(
        token_rows,
        lax.all_gather(out_weight, "tp", axis=0, tiled=True),
        preferred_element_type=jnp.float32,
    )
    stream_wide = (tokens.astype(jnp.float32) + projected).astype(jnp.bfloat16).astype(jnp.float32)
    inverse = lax.rsqrt(jnp.mean(stream_wide * stream_wide, axis=1, keepdims=True) + 1e-05)
    normed = (stream_wide * inverse * norm_gain[None, :]).astype(jnp.bfloat16)
    n_experts = gate_weight.shape[0] * sp_count
    top_count = expert_ids.shape[1]
    capacity = max(2, 3 * tok_dev * top_count // (2 * n_experts))
    flat_ids = expert_ids.reshape(-1)
    hits = (flat_ids[:, None] == jnp.arange(n_experts, dtype=jnp.int32)[None, :]).astype(jnp.int32)
    earlier = jnp.cumsum(hits, axis=0) - hits
    slot_index = flat_ids * capacity + jnp.sum(earlier * hits, axis=1)
    placement_map = (
        jnp.arange(n_experts * capacity, dtype=jnp.int32)[:, None] == slot_index[None, :]
    ).astype(jnp.bfloat16)
    repeated = jnp.repeat(normed, top_count, axis=0)
    dispatch = jnp.dot(placement_map, repeated, preferred_element_type=jnp.float32).astype(
        jnp.bfloat16
    )
    dispatch = dispatch.reshape(n_experts, capacity, model_width)
    arrived = lax.all_to_all(dispatch, "sp", split_axis=0, concat_axis=0, tiled=True)
    row_block = arrived.reshape(-1, model_width)
    rows_in = lax.all_gather(row_block, "tp", axis=0, tiled=True)
    gate_value = jnp.dot(rows_in, gate_weight[0], preferred_element_type=jnp.float32)
    up_value = jnp.dot(rows_in, up_weight[0], preferred_element_type=jnp.float32)
    hidden = (jax.nn.silu(gate_value) * up_value).astype(jnp.bfloat16)
    summed = lax.psum_scatter(
        jnp.dot(hidden, down_weight[0], preferred_element_type=jnp.float32).astype(jnp.bfloat16),
        "tp",
        scatter_dimension=0,
        tiled=True,
    )
    returned = summed.reshape(arrived.shape)
    back = lax.all_to_all(returned, "sp", split_axis=0, concat_axis=0, tiled=True)
    flat_back = back.reshape(n_experts * capacity, model_width)
    picked = flat_back[slot_index].astype(jnp.float32).reshape(tok_dev, top_count, model_width)
    mixture = jnp.sum(picked * route_weights[:, :, None], axis=1)
    return (stream_wide + mixture).astype(jnp.bfloat16)


def solution(mesh):
    in_specs = (
        P(("sp", "tp"), None),
        P("sp", "tp"),
        P("sp", "tp"),
        P("sp", "tp"),
        P("sp", "tp"),
        P("tp", None),
        P(),
        P("sp", None, "tp"),
        P("sp", None, "tp"),
        P("sp", "tp", None),
        P(("sp", "tp"), None),
        P(("sp", "tp"), None),
    )
    out_specs = P(("sp", "tp"), None)
    return jax.shard_map(shards, mesh=mesh, in_specs=in_specs, out_specs=out_specs, check_vma=False)
```

profile of v0, /device:TPU:2, one launch (start us, length us, event | category | flops | bytes accessed | tf_op | source)
XLA Modules:
  0.0 335.4 jit_solution(8175806650671181984)
XLA Ops:
  6.5 1.8 pad_maximum_fusion
  8.4 0.0 all-gather.4.cloned.1.call-update
  8.4 0.0 all-gather.6.cloned.1.call-start
  8.4 0.7 all-gather.6.cloned.1.call-update
  9.2 1.3 broadcast_in_dim.61
  10.5 7.5 %all-to-all-start = ((f32[16,512,2]{1,2,0:T(2,128)}), f32[16,512,2]{1,2,0:T(2,128)S(1)}, u32[]{:S(2)}, u32[]{:S(2)}) async-start(f32[16,512,2]{1,2,0:T(2,128)} %broadcast_in_dim.61), calls=%async_computation | async-start | bytes 131072 | tf_op jit(solution)/shard_map/all_to_all | solution.py:12
  18.0 1.0 copy.28
  19.0 0.8 copy.33
  19.7 0.1 reshape.143
  19.8 0.1 fusion.26
  19.9 0.1 reduce_window_sum.11
  20.0 49.1 %all-gather.4.cloned.1.call-done = bf16[8192,256]{1,0:T(8,128)(2,1)} async-done(((bf16[512,256]{1,0:T(8,128)(2,1)}), bf16[8192,256]{1,0:T(8,128)(2,1)}) %all-gather.4.cloned.1.call-update) | async-done | bytes 4194320 | tf_op jit(solution)/shard_map/all_gather | solution.py:31
  69.2 4.4 %fusion.30 = (bf16[8192,128]{1,0:T(8,128)(2,1)}, bf16[8192,128]{1,0:T(8,128)(2,1)}) fusion(bf16[8192,256]{1,0:T(8,128)(2,1)} %all-gather.4.cloned.1.call-done), kind=kLoop, calls=%fused_computation.54 | loop fusion | bytes 8388608 | tf_op jit(solution)/shard_map/split | solution.py:32
  73.6 3.9 %copy.29 = bf16[8,1024,128]{1,2,0:T(8,128)(2,1)} copy(bf16[8,1024,128]{2,1,0:T(8,128)(2,1)} %bitcast.60) | data formatting | bytes 4194304
  77.5 3.9 %copy.30 = bf16[8,1024,128]{1,2,0:T(8,128)(2,1)} copy(bf16[8,1024,128]{2,1,0:T(8,128)(2,1)} %bitcast.59) | data formatting | bytes 4194304
  81.5 16.5 %while.15 = (s32[]{:T(128)}, f32[2,512]{1,0:T(2,128)S(1)}, f32[2,512]{1,0:T(2,128)S(1)}, f32[2,512,64]{1,2,0:T(8,128)S(1)}, s32[8]{0:T(128)S(1)}, /*index=5*/s32...) while((s32[]{:T(128)}, f32[2,512]{1,0:T(2,128)S(1)}, ...), condition=%wide.region_5.6_spmd.clone, body=%wide.region_0.5_spmd.clone.sunk | while | flops 289017344 | bytes 17043828 | solution.py:113
  81.5 0.6 dynamic_slice.31
  82.8 6.2 %conditional.3 = ((f32[2,512]{1,0:T(2,128)S(1)}, f32[2,512]{1,0:T(2,128)S(1)}, f32[2,512,64]{1,2,0:T(8,128)S(1)})) conditional(s32[]{:T(128)} %convert_element_type.83, (f32[2,512]{1,0:T(2,128)S(1)}, f32[2,512]{1,0:T(2,128)S(1)}, f32[2,512,64]{1,2,0:T(8,128)S(1)}) %tuple.43, (s32[]{:T(128)}, s32[]{:T(128)}, bf16[8,1024,128]{1,2,0:T(8,128)(2,1)}, ...), branch_computations={%region_1.1_spmd, %region_2.4_spmd} | conditional | flops 289017344 | bytes 17041490 | solution.py:111
  82.8 0.1 dynamic-slice_bitcast_fusion
  82.9 0.4 broadcast_compare_fusion
  83.3 1.1 constant_dynamic-slice_fusion
  84.3 1.4 fusion.4
  85.7 1.5 fusion.3
  87.2 1.7 fusion.8
  89.0 0.6 dynamic_slice.31
  90.3 0.6 dynamic_slice.31
  91.6 0.6 dynamic_slice.31
  92.9 0.6 dynamic_slice.31
  94.2 0.6 dynamic_slice.31
  95.5 0.6 dynamic_slice.31
  96.7 0.6 dynamic_slice.31
  98.1 0.2 copy.31
  98.2 0.8 all_to_all.24
  99.0 7.1 %all-to-all-start.1 = ((bf16[16,32,128]{2,1,0:T(8,128)(2,1)}), bf16[16,32,128]{2,1,0:T(8,128)(2,1)S(1)}, u32[]{:S(2)}, u32[]{:S(2)}) async-start(bf16[16,32,128]{2,1,0:T(8,128)(2,1)} %all_to_all.24), calls=%async_computation.1 | async-start | bytes 262144 | tf_op jit(solution)/shard_map/all_to_all | solution.py:121
  106.1 0.0 all-gather.8.cloned.1.call-start
  106.2 0.2 select_reduce_fusion
  106.4 10.4 %all-to-all-done.1 = bf16[16,32,128]{2,1,0:T(8,128)(2,1)S(1)} async-done(((bf16[16,32,128]{2,1,0:T(8,128)(2,1)}), bf16[16,32,128]{2,1,0:T(8,128)(2,1)S(1)}, u32[]{:S(2)}, u32[]{:S(2)}) %all-to-all-start.1) | async-done | bytes 131104 | tf_op jit(solution)/shard_map/all_to_all | solution.py:121
  116.8 12.6 %all-gather.6.cloned.1.call-done = bf16[2048,2048]{1,0:T(8,128)(2,1)} async-done(((bf16[128,2048]{1,0:T(8,128)(2,1)}), bf16[2048,2048]{1,0:T(8,128)(2,1)}) %all-gather.6.cloned.1.call-update) | async-done | bytes 8388624 | tf_op jit(solution)/shard_map/all_gather | solution.py:124
  129.4 5.0 %multiply_reduce_fusion.1 = (f32[32]{0:T(128)S(1)}, f32[32,2048]{1,0:T(8,128)S(1)}) fusion(bf16[2048,2048]{1,0:T(8,128)(2,1)} %all-gather.6.cloned.1.call-done, bf16[32,2048]{1,0:T(8,128)(2,1)S(1)} %copy-done.2, bf16[16,32,128]{2,1,0:T(8,128)(2,1)S(1)} %all-to-all-done.1), kind=kOutput, calls=%fused_computation.36 | convolution fusion | flops 268828640 | bytes 8913024 | tf_op jit(solution)/shard_map/dot_general | solution.py:122
  134.5 0.1 multiply_convert_fusion
  134.6 0.1 broadcast_in_dim.62
  134.7 0.1 reshape.144
  134.9 0.2 convolution_convert_fusion.1
  135.1 0.1 reshape.145
  135.2 44.9 %all_to_all.34 = bf16[16,6,2048]{2,1,0:T(8,128)(2,1)S(1)} all-to-all(bf16[16,6,2048]{2,1,0:T(8,128)(2,1)S(1)} %reshape.145), channel_id=1, replica_groups=mesh['sp'=16,'tp'=16] {'sp'}, dimensions={0} | all-to-all | bytes 786432 | tf_op jit(solution)/shard_map/all_to_all | solution.py:145
  180.1 0.9 reshape.146
  181.0 0.0 all-gather.8.cloned.1.call-update
  181.1 0.2 reduce-scatter.2.cloned.1.call-start
  181.3 40.0 %all-gather.8.cloned.1.call-done = bf16[1536,2048]{1,0:T(8,128)(2,1)} async-done(((bf16[96,2048]{1,0:T(8,128)(2,1)}), bf16[1536,2048]{1,0:T(8,128)(2,1)}) %all-gather.8.cloned.1.call-update) | async-done | bytes 6291472 | tf_op jit(solution)/shard_map/all_gather | solution.py:147
  221.2 7.9 %fusion.19 = f32[1536,448]{0,1:T(8,128)} fusion(bf16[1536,2048]{1,0:T(8,128)(2,1)} %all-gather.8.cloned.1.call-done, bf16[1,2048,448]{1,2,0:T(8,128)(2,1)} %param.23), kind=kOutput, calls=%fused_computation.30 | convolution fusion | flops 2818572288 | bytes 10878976 | tf_op jit(solution)/shard_map/dot_general | solution.py:148
  229.1 13.2 %convolution_convert_fusion = bf16[1536,2048]{1,0:T(8,128)(2,1)} fusion(bf16[1,448,2048]{2,1,0:T(8,128)(2,1)S(1)} %copy-done, bf16[1536,2048]{1,0:T(8,128)(2,1)} %all-gather.8.cloned.1.call-done, f32[1536,448]{0,1:T(8,128)} %fusion.19, bf16[1,2048,448]{1,2,0:T(8,128)(2,1)} %param.24), kind=kOutput, calls=%fused_computation.21 | convolution fusion | flops 5644419072 | bytes 19005440 | tf_op jit(solution)/shard_map/dot_general | solution.py:152
  242.3 0.0 reduce-scatter.2.cloned.1.call-update
  242.3 65.9 %reduce-scatter.2.cloned.1.call-done = bf16[96,2048]{1,0:T(8,128)(2,1)} async-done(((bf16[1536,2048]{1,0:T(8,128)(2,1)}), bf16[96,2048]{1,0:T(8,128)(2,1)}) %reduce-scatter.2.cloned.1.call-update) | async-done | bytes 393232 | tf_op jit(solution)/shard_map/reduce_scatter | solution.py:151
  308.2 1.9 reshape.147
  310.2 7.2 %all-to-all-start.3 = ((bf16[16,6,2048]{2,1,0:T(8,128)(2,1)}), bf16[16,6,2048]{2,1,0:T(8,128)(2,1)S(1)}, u32[]{:S(2)}, u32[]{:S(2)}) async-start(bf16[16,6,2048]{2,1,0:T(8,128)(2,1)} %reshape.147), calls=%async_computation.4 | async-start | bytes 1048576 | tf_op jit(solution)/shard_map/all_to_all | solution.py:158
  317.4 0.1 copy.34
  317.5 0.1 mul.106
  317.6 0.1 copy.35
  317.7 8.5 %all-to-all-done.3 = bf16[16,6,2048]{2,1,0:T(8,128)(2,1)S(1)} async-done(((bf16[16,6,2048]{2,1,0:T(8,128)(2,1)}), bf16[16,6,2048]{2,1,0:T(8,128)(2,1)S(1)}, u32[]{:S(2)}, u32[]{:S(2)}) %all-to-all-start.3) | async-done | bytes 393248 | tf_op jit(solution)/shard_map/all_to_all | solution.py:158
  326.2 0.1 reshape.148
  326.3 0.7 gather_fusion
  327.1 0.3 reshape.149
  327.4 0.7 multiply_reduce_fusion
  328.1 0.7 add_convert_fusion
  (44 shorter events, 0.2 us)
Async XLA Ops:
  6.5 222.6 %copy-start = (bf16[1,448,2048]{2,1,0:T(8,128)(2,1)S(1)}, bf16[1,448,2048]{2,1,0:T(8,128)(2,1)}, u32[]{:S(2)}) copy-start(bf16[1,448,2048]{2,1,0:T(8,128)(2,1)} %param.25) | copy-start | bytes 5505028
  6.5 62.6 %all-gather.4.cloned.1.call-start = ((), (), s32[]{:S(2)}) async-start(), calls=%async_computation.5 | async-start | bytes 4456448 | tf_op jit(solution)/shard_map/all_gather | solution.py:31
  8.4 121.0 %all-gather.6.cloned.1.call-start = ((), (), s32[]{:S(2)}) async-start(), calls=%async_computation.6 | async-start | bytes 8912896 | tf_op jit(solution)/shard_map/all_gather | solution.py:124
  10.5 70.9 %all-to-all-start = ((f32[16,512,2]{1,2,0:T(2,128)}), f32[16,512,2]{1,2,0:T(2,128)S(1)}, u32[]{:S(2)}, u32[]{:S(2)}) async-start(f32[16,512,2]{1,2,0:T(2,128)} %broadcast_in_dim.61), calls=%async_computation | async-start | bytes 131072 | tf_op jit(solution)/shard_map/all_to_all | solution.py:12
  73.6 7.9 %copy-start.1 = (f32[512,2]{0,1:T(2,128)S(1)}, f32[512,2]{0,1:T(2,128)}, u32[]{:S(2)}) copy-start(f32[512,2]{0,1:T(2,128)} %param.20) | copy-start | bytes 12292
  81.5 47.9 %copy-start.2 = (bf16[32,2048]{1,0:T(8,128)(2,1)S(1)}, bf16[32,2048]{1,0:T(8,128)(2,1)}, u32[]{:S(2)}) copy-start(bf16[32,2048]{1,0:T(8,128)(2,1)} %param.16) | copy-start | bytes 393220
  99.0 17.7 %all-to-all-start.1 = ((bf16[16,32,128]{2,1,0:T(8,128)(2,1)}), bf16[16,32,128]{2,1,0:T(8,128)(2,1)S(1)}, u32[]{:S(2)}, u32[]{:S(2)}) async-start(bf16[16,32,128]{2,1,0:T(8,128)(2,1)} %all_to_all.24), calls=%async_computation.1 | async-start | bytes 262144 | tf_op jit(solution)/shard_map/all_to_all | solution.py:121
  106.1 115.1 %all-gather.8.cloned.1.call-start = ((), (), s32[]{:S(2)}) async-start(), calls=%async_computation.7 | async-start | bytes 6684672 | tf_op jit(solution)/shard_map/all_gather | solution.py:147
  106.4 28.1 %copy-start.3 = (f32[2048]{0:T(1024)S(1)}, f32[2048]{0:T(1024)}, u32[]{:S(2)}) copy-start(f32[2048]{0:T(1024)} %param.22) | copy-start | bytes 24580
  181.1 127.2 %reduce-scatter.2.cloned.1.call-start = ((), (), s32[]{:S(2)}) async-start(), calls=%async_computation.8 | async-start | bytes 6684672 | tf_op jit(solution)/shard_map/reduce_scatter | solution.py:151
  242.3 75.1 %copy-start.4 = (s32[32,2]{0,1:T(2,128)S(1)}, s32[32,2]{0,1:T(2,128)}, u32[]{:S(2)}) copy-start(s32[32,2]{0,1:T(2,128)} %param.26) | copy-start | bytes 772
  242.3 75.3 %copy-start.5 = (f32[32,2]{0,1:T(2,128)S(1)}, f32[32,2]{0,1:T(2,128)}, u32[]{:S(2)}) copy-start(f32[32,2]{0,1:T(2,128)} %param.27) | copy-start | bytes 772
  310.2 16.0 %all-to-all-start.3 = ((bf16[16,6,2048]{2,1,0:T(8,128)(2,1)}), bf16[16,6,2048]{2,1,0:T(8,128)(2,1)S(1)}, u32[]{:S(2)}, u32[]{:S(2)}) async-start(bf16[16,6,2048]{2,1,0:T(8,128)(2,1)} %reshape.147), calls=%async_computation.4 | async-start | bytes 1048576 | tf_op jit(solution)/shard_map/all_to_all | solution.py:158
Sparse Core Ops, SparseCore 0:
  9.8 59.3 all-gather.3
  71.0 58.3 all-gather.5
  181.2 40.0 all-gather.7
  242.5 65.7 reduce-scatter.1
where the time goes:
time: 336 us; the launch traced here: 335 us
  waiting for transfers between devices  187 us (56%)
  blocking collectives  44.9 us (13%)
  matrix products  29.4 us (9%)
  local copies, waits for them, and re-layouts  27.1 us (8%)
  starting transfers between devices  22.1 us (7%)
  between operations  13.3 us (4%)
  loops' own time  5.68 us (2%)
  other arithmetic  5.62 us (2%)
    reduce_scatter x1, waiting for transfers between devices, shards(): lax.psum_scatter(jnp.dot(hidden, down_weight[0], preferred_element_type=j...  65.9 us
    all_gather x1, waiting for transfers between devices, sent_together(): filled = lax.all_gather(both, axis, axis=dim, tiled=True)  49.1 us
    all_to_all x1, blocking collectives, shards(): lax.all_to_all(dispatch, 'sp', split_axis=0, concat_axis=0, tiled=True)  44.9 us
    all_gather x1, waiting for transfers between devices, shards(): rows_in = lax.all_gather(row_block, 'tp', axis=0, tiled=True)  40 us
    dot_general x1, matrix products, shards(): jnp.dot(hidden, down_weight[0], preferred_element_type=jnp.float32)  13.2 us
    all_gather x1, waiting for transfers between devices, shards(): lax.all_gather(out_weight, 'tp', axis=0, tiled=True)  12.6 us
    all_to_all x1, waiting for transfers between devices, shards(): lax.all_to_all(attended, 'tp', split_axis=0, concat_axis=1, tiled=True)  10.4 us
    unnamed x17, local copies, waits for them, and re-layouts  9.73 us
  transfers between devices with their start and end apart: 7, of which 6 were waited for; matrix products, arithmetic and copies ran while one was open for 8% of the time, Pallas kernels for 0%

commit v1 on v0

--- a/solution.py
+++ b/solution.py
@@ -144,7 +144,21 @@
     dispatch = dispatch.reshape(n_experts, capacity, model_width)
     arrived = lax.all_to_all(dispatch, "sp", split_axis=0, concat_axis=0, tiled=True)
     row_block = arrived.reshape(-1, model_width)
-    rows_in = lax.all_gather(row_block, "tp", axis=0, tiled=True)
+    ways, here, turn = (lax.axis_size("tp"), lax.axis_index("tp"), row_block.shape[0])
+    dims_2 = [n * ways if d == 0 else n for d, n in enumerate(row_block.shape)]
+    full = lax.dynamic_update_slice_in_dim(
+        jnp.zeros(dims_2, row_block.dtype), row_block, here * turn, axis=0
+    )
+    going_up = going_down = row_block
+    for far in range(1, ways // 2 + 1):
+        going_up = lax.ppermute(going_up, "tp", [(d, (d + 1) % ways) for d in range(ways)])
+        full = lax.dynamic_update_slice_in_dim(full, going_up, (here - far) % ways * turn, axis=0)
+        if 2 * far < ways:
+            going_down = lax.ppermute(going_down, "tp", [(d, (d - 1) % ways) for d in range(ways)])
+            full = lax.dynamic_update_slice_in_dim(
+                full, going_down, (here + far) % ways * turn, axis=0
+            )
+    rows_in = full
     gate_value = jnp.dot(rows_in, gate_weight[0], preferred_element_type=jnp.float32)
     up_value = jnp.dot(rows_in, up_weight[0], preferred_element_type=jnp.float32)
     hidden = (jax.nn.silu(gate_value) * up_value).astype(jnp.bfloat16)

time: 336 us -> 357 us (1.062)
  starting transfers between devices: 22.1 us -> 42.6 us
    ppermute x0 -> x15, waiting for transfers between devices: none -> 45.2 us  [the longest x8 45.1 us: shards(): lax.ppermute(going_up, 'tp', [(d, (d + 1) % ways) for d in range(ways)])]
    all_gather x1 -> x0, waiting for transfers between devices: 40 us -> none  [shards(): rows_in = lax.all_gather(row_block, 'tp', axis=0, tiled=True)]
    ppermute x0 -> x15, starting transfers between devices: none -> 20.7 us  [the longest x7 20.7 us: shards(): lax.ppermute(going_down, 'tp', [(d, (d - 1) % ways) for d in range(ways)])]
    reduce_scatter x1, waiting for transfers between devices: 65.9 us -> 61.2 us  [shards(): lax.psum_scatter(jnp.dot(hidden, down_weight[0], preferred_element_type=j...]
    unnamed x17 -> x21, local copies, waits for them, and re-layouts: 9.73 us -> 12.4 us
  transfers between devices with their start and end apart: 7 -> 21, of which waited for: 6 -> 13; matrix products, arithmetic and copies ran while one was open for 8% -> 8% of each run, Pallas kernels for 0% -> 0%
where the time goes in v1:
time: 357 us; the launch traced here: 356 us
  waiting for transfers between devices  188 us (53%)
  blocking collectives  44.9 us (13%)
  starting transfers between devices  42.6 us (12%)
  local copies, waits for them, and re-layouts  30.3 us (8%)
  matrix products  26.1 us (7%)
  between operations  13.5 us (4%)
  loops' own time  5.68 us (2%)
  other arithmetic  5.62 us (2%)
    reduce_scatter x1, waiting for transfers between devices, shards(): lax.psum_scatter(jnp.dot(hidden, down_weight[0], preferred_element_type=j...  61.2 us
    all_gather x1, waiting for transfers between devices, sent_together(): filled = lax.all_gather(both, axis, axis=dim, tiled=True)  49.1 us
    ppermute x8, waiting for transfers between devices, shards(): lax.ppermute(going_up, 'tp', [(d, (d + 1) % ways) for d in range(ways)])  45.1 us
    all_to_all x1, blocking collectives, shards(): lax.all_to_all(dispatch, 'sp', split_axis=0, concat_axis=0, tiled=True)  44.9 us
    ppermute x7, starting transfers between devices, shards(): lax.ppermute(going_down, 'tp', [(d, (d - 1) % ways) for d in range(ways)])  20.7 us
    dot_general x1, matrix products, shards(): jnp.dot(hidden, down_weight[0], preferred_element_type=jnp.float32)  13.2 us
    all_gather x1, waiting for transfers between devices, shards(): lax.all_gather(out_weight, 'tp', axis=0, tiled=True)  12.6 us
    unnamed x21, local copies, waits for them, and re-layouts  12.4 us
  transfers between devices with their start and end apart: 21, of which 13 were waited for; matrix products, arithmetic and copies ran while one was open for 8% of the time, Pallas kernels for 0%

profile of v1, /device:TPU:2, one launch (start us, length us, event | category | flops | bytes accessed | tf_op | source)
XLA Modules:
  0.0 356.4 jit_solution(4255688769475281938)
XLA Ops:
  6.5 1.8 pad_maximum_fusion
  8.5 0.7 all-gather.5.cloned.1.call-update
  9.2 1.3 broadcast_in_dim.64
  10.5 7.5 %all-to-all-start = ((f32[16,512,2]{1,2,0:T(2,128)}), f32[16,512,2]{1,2,0:T(2,128)S(1)}, u32[]{:S(2)}, u32[]{:S(2)}) async-start(f32[16,512,2]{1,2,0:T(2,128)} %broadcast_in_dim.64), calls=%async_computation | async-start | bytes 131072 | tf_op jit(solution)/shard_map/all_to_all | solution.py:12
  18.0 1.0 copy.28
  19.0 0.8 copy.33
  20.0 49.1 %all-gather.3.cloned.1.call-done = bf16[8192,256]{1,0:T(8,128)(2,1)} async-done(((bf16[512,256]{1,0:T(8,128)(2,1)}), bf16[8192,256]{1,0:T(8,128)(2,1)}) %all-gather.3.cloned.1.call-update) | async-done | bytes 4194320 | tf_op jit(solution)/shard_map/all_gather | solution.py:31
  69.2 4.4 %fusion.32 = (bf16[8192,128]{1,0:T(8,128)(2,1)}, bf16[8192,128]{1,0:T(8,128)(2,1)}) fusion(bf16[8192,256]{1,0:T(8,128)(2,1)} %all-gather.3.cloned.1.call-done), kind=kLoop, calls=%fused_computation.70 | loop fusion | bytes 8388608 | tf_op jit(solution)/shard_map/split | solution.py:32
  73.6 4.0 %copy.29 = bf16[8,1024,128]{1,2,0:T(8,128)(2,1)} copy(bf16[8,1024,128]{2,1,0:T(8,128)(2,1)} %bitcast.62) | data formatting | bytes 4194304
  77.6 3.9 %copy.30 = bf16[8,1024,128]{1,2,0:T(8,128)(2,1)} copy(bf16[8,1024,128]{2,1,0:T(8,128)(2,1)} %bitcast.61) | data formatting | bytes 4194304
  81.6 16.5 %while.15 = (s32[]{:T(128)}, f32[2,512]{1,0:T(2,128)S(1)}, f32[2,512]{1,0:T(2,128)S(1)}, f32[2,512,64]{1,2,0:T(8,128)S(1)}, s32[8]{0:T(128)S(1)}, /*index=5*/s32...) while((s32[]{:T(128)}, f32[2,512]{1,0:T(2,128)S(1)}, ...), condition=%wide.region_5.6_spmd.clone, body=%wide.region_0.5_spmd.clone.sunk | while | flops 289017344 | bytes 17043828 | solution.py:113
  81.6 0.6 dynamic_slice.31
  82.8 6.2 %conditional.3 = ((f32[2,512]{1,0:T(2,128)S(1)}, f32[2,512]{1,0:T(2,128)S(1)}, f32[2,512,64]{1,2,0:T(8,128)S(1)})) conditional(s32[]{:T(128)} %convert_element_type.83, (f32[2,512]{1,0:T(2,128)S(1)}, f32[2,512]{1,0:T(2,128)S(1)}, f32[2,512,64]{1,2,0:T(8,128)S(1)}) %tuple.43, (s32[]{:T(128)}, s32[]{:T(128)}, bf16[8,1024,128]{1,2,0:T(8,128)(2,1)}, ...), branch_computations={%region_1.1_spmd, %region_2.4_spmd} | conditional | flops 289017344 | bytes 17041490 | solution.py:111
  82.9 0.4 broadcast_compare_fusion
  83.3 1.1 constant_dynamic-slice_fusion
  84.4 1.4 fusion.4
  85.8 1.5 fusion.3
  87.3 1.7 fusion.8
  89.0 0.6 dynamic_slice.31
  90.3 0.6 dynamic_slice.31
  91.6 0.6 dynamic_slice.31
  92.9 0.6 dynamic_slice.31
  94.2 0.6 dynamic_slice.31
  95.5 0.6 dynamic_slice.31
  96.8 0.6 dynamic_slice.31
  98.1 0.2 copy.31
  98.3 0.8 all_to_all.24
  99.1 7.1 %all-to-all-start.1 = ((bf16[16,32,128]{2,1,0:T(8,128)(2,1)}), bf16[16,32,128]{2,1,0:T(8,128)(2,1)S(1)}, u32[]{:S(2)}, u32[]{:S(2)}) async-start(bf16[16,32,128]{2,1,0:T(8,128)(2,1)} %all_to_all.24), calls=%async_computation.1 | async-start | bytes 262144 | tf_op jit(solution)/shard_map/all_to_all | solution.py:121
  106.2 0.2 select_reduce_fusion
  106.4 10.3 %all-to-all-done.1 = bf16[16,32,128]{2,1,0:T(8,128)(2,1)S(1)} async-done(((bf16[16,32,128]{2,1,0:T(8,128)(2,1)}), bf16[16,32,128]{2,1,0:T(8,128)(2,1)S(1)}, u32[]{:S(2)}, u32[]{:S(2)}) %all-to-all-start.1) | async-done | bytes 131104 | tf_op jit(solution)/shard_map/all_to_all | solution.py:121
  116.8 12.6 %all-gather.5.cloned.1.call-done = bf16[2048,2048]{1,0:T(8,128)(2,1)} async-done(((bf16[128,2048]{1,0:T(8,128)(2,1)}), bf16[2048,2048]{1,0:T(8,128)(2,1)}) %all-gather.5.cloned.1.call-update) | async-done | bytes 8388624 | tf_op jit(solution)/shard_map/all_gather | solution.py:124
  129.4 5.0 %multiply_reduce_fusion.1 = (f32[32]{0:T(128)S(1)}, f32[32,2048]{1,0:T(8,128)S(1)}) fusion(bf16[2048,2048]{1,0:T(8,128)(2,1)} %all-gather.5.cloned.1.call-done, bf16[32,2048]{1,0:T(8,128)(2,1)S(1)} %copy-done.3, bf16[16,32,128]{2,1,0:T(8,128)(2,1)S(1)} %all-to-all-done.1), kind=kOutput, calls=%fused_computation.36 | convolution fusion | flops 268828640 | bytes 8913024 | tf_op jit(solution)/shard_map/dot_general | solution.py:122
  134.6 0.1 broadcast_in_dim.66
  134.9 0.2 convolution_convert_fusion.1
  135.1 0.1 reshape.145
  135.2 44.9 %all_to_all.34 = bf16[16,6,2048]{2,1,0:T(8,128)(2,1)S(1)} all-to-all(bf16[16,6,2048]{2,1,0:T(8,128)(2,1)S(1)} %reshape.145), channel_id=1, replica_groups=mesh['sp'=16,'tp'=16] {'sp'}, dimensions={0} | all-to-all | bytes 786432 | tf_op jit(solution)/shard_map/all_to_all | solution.py:145
  180.1 0.1 reshape.146
  180.3 2.9 collective-permute-start.1
  183.2 0.8 broadcast_in_dim.65
  184.1 4.6 %collective-permute-done = bf16[96,2048]{1,0:T(8,128)(2,1)S(1)} collective-permute-done((bf16[96,2048]{1,0:T(8,128)(2,1)S(1)}, bf16[96,2048]{1,0:T(8,128)(2,1)S(1)}, u32[]{:S(2)}, u32[]{:S(2)}) %collective-permute-start) | collective-permute-done | bytes 393248 | tf_op jit(solution)/shard_map/ppermute | solution.py:154
  188.7 3.0 collective-permute-start.3
  191.8 5.4 %collective-permute-done.2 = bf16[96,2048]{1,0:T(8,128)(2,1)S(1)} collective-permute-done((bf16[96,2048]{1,0:T(8,128)(2,1)S(1)}, bf16[96,2048]{1,0:T(8,128)(2,1)S(1)}, u32[]{:S(2)}, u32[]{:S(2)}) %collective-permute-start.2) | collective-permute-done | bytes 393248 | tf_op jit(solution)/shard_map/ppermute | solution.py:154
  197.1 3.0 collective-permute-start.5
  200.2 5.4 %collective-permute-done.4 = bf16[96,2048]{1,0:T(8,128)(2,1)S(1)} collective-permute-done((bf16[96,2048]{1,0:T(8,128)(2,1)S(1)}, bf16[96,2048]{1,0:T(8,128)(2,1)S(1)}, u32[]{:S(2)}, u32[]{:S(2)}) %collective-permute-start.4) | collective-permute-done | bytes 393248 | tf_op jit(solution)/shard_map/ppermute | solution.py:154
  205.5 3.0 collective-permute-start.7
  208.6 5.4 %collective-permute-done.6 = bf16[96,2048]{1,0:T(8,128)(2,1)S(1)} collective-permute-done((bf16[96,2048]{1,0:T(8,128)(2,1)S(1)}, bf16[96,2048]{1,0:T(8,128)(2,1)S(1)}, u32[]{:S(2)}, u32[]{:S(2)}) %collective-permute-start.6) | collective-permute-done | bytes 393248 | tf_op jit(solution)/shard_map/ppermute | solution.py:154
  213.9 3.0 collective-permute-start.9
  217.0 5.4 %collective-permute-done.8 = bf16[96,2048]{1,0:T(8,128)(2,1)S(1)} collective-permute-done((bf16[96,2048]{1,0:T(8,128)(2,1)S(1)}, bf16[96,2048]{1,0:T(8,128)(2,1)S(1)}, u32[]{:S(2)}, u32[]{:S(2)}) %collective-permute-start.8) | collective-permute-done | bytes 393248 | tf_op jit(solution)/shard_map/ppermute | solution.py:154
  222.4 3.0 collective-permute-start.11
  225.4 5.4 %collective-permute-done.10 = bf16[96,2048]{1,0:T(8,128)(2,1)S(1)} collective-permute-done((bf16[96,2048]{1,0:T(8,128)(2,1)S(1)}, bf16[96,2048]{1,0:T(8,128)(2,1)S(1)}, u32[]{:S(2)}, u32[]{:S(2)}) %collective-permute-start.10) | collective-permute-done | bytes 393248 | tf_op jit(solution)/shard_map/ppermute | solution.py:154
  230.8 3.0 collective-permute-start.13
  233.8 5.4 %collective-permute-done.12 = bf16[96,2048]{1,0:T(8,128)(2,1)S(1)} collective-permute-done((bf16[96,2048]{1,0:T(8,128)(2,1)S(1)}, bf16[96,2048]{1,0:T(8,128)(2,1)S(1)}, u32[]{:S(2)}, u32[]{:S(2)}) %collective-permute-start.12) | collective-permute-done | bytes 393248 | tf_op jit(solution)/shard_map/ppermute | solution.py:154
  239.3 8.3 %collective-permute-done.14 = bf16[96,2048]{1,0:T(8,128)(2,1)S(1)} collective-permute-done((bf16[96,2048]{1,0:T(8,128)(2,1)S(1)}, bf16[96,2048]{1,0:T(8,128)(2,1)S(1)}, u32[]{:S(2)}, u32[]{:S(2)}) %collective-permute-start.14) | collective-permute-done | bytes 393248 | tf_op jit(solution)/shard_map/ppermute | solution.py:154
  247.6 2.6 copy-done.1
  250.2 4.6 %fusion.21 = f32[1536,448]{0,1:T(8,128)} fusion(bf16[1536,2048]{1,0:T(8,128)(2,1)S(1)} %constant_dynamic-update-slice_fusion, bf16[1,2048,448]{1,2,0:T(8,128)(2,1)S(1)} %copy-done.7), kind=kOutput, calls=%fused_computation.30 | convolution fusion | flops 2818572288 | bytes 10878976 | tf_op jit(solution)/shard_map/dot_general | solution.py:162
  254.8 13.2 %convolution_convert_fusion = bf16[1536,2048]{1,0:T(8,128)(2,1)} fusion(bf16[1,448,2048]{2,1,0:T(8,128)(2,1)S(1)} %copy-done, f32[1536,448]{0,1:T(8,128)} %fusion.21, bf16[1536,2048]{1,0:T(8,128)(2,1)} %copy-done.1, bf16[1,2048,448]{1,2,0:T(8,128)(2,1)} %param.24), kind=kOutput, calls=%fused_computation.21 | convolution fusion | flops 5644419072 | bytes 19005440 | tf_op jit(solution)/shard_map/dot_general | solution.py:166
  268.1 61.2 %reduce-scatter.2.cloned.1.call-done = bf16[96,2048]{1,0:T(8,128)(2,1)} async-done(((bf16[1536,2048]{1,0:T(8,128)(2,1)}), bf16[96,2048]{1,0:T(8,128)(2,1)}) %reduce-scatter.2.cloned.1.call-update) | async-done | bytes 393232 | tf_op jit(solution)/shard_map/reduce_scatter | solution.py:165
  329.3 1.9 reshape.147
  331.2 7.3 %all-to-all-start.3 = ((bf16[16,6,2048]{2,1,0:T(8,128)(2,1)}), bf16[16,6,2048]{2,1,0:T(8,128)(2,1)S(1)}, u32[]{:S(2)}, u32[]{:S(2)}) async-start(bf16[16,6,2048]{2,1,0:T(8,128)(2,1)} %reshape.147), calls=%async_computation.4 | async-start | bytes 1048576 | tf_op jit(solution)/shard_map/all_to_all | solution.py:172
  338.8 8.5 %all-to-all-done.3 = bf16[16,6,2048]{2,1,0:T(8,128)(2,1)S(1)} async-done(((bf16[16,6,2048]{2,1,0:T(8,128)(2,1)}), bf16[16,6,2048]{2,1,0:T(8,128)(2,1)S(1)}, u32[]{:S(2)}, u32[]{:S(2)}) %all-to-all-start.3) | async-done | bytes 393248 | tf_op jit(solution)/shard_map/all_to_all | solution.py:172
  347.4 0.7 gather_fusion
  348.1 0.3 reshape.149
  348.5 0.7 multiply_reduce_fusion
  349.2 0.7 add_convert_fusion
  (92 shorter events, 1.9 us)
Async XLA Ops:
  6.5 248.3 %copy-start = (bf16[1,448,2048]{2,1,0:T(8,128)(2,1)S(1)}, bf16[1,448,2048]{2,1,0:T(8,128)(2,1)}, u32[]{:S(2)}) copy-start(bf16[1,448,2048]{2,1,0:T(8,128)(2,1)} %param.25) | copy-start | bytes 5505028
  6.5 62.6 %all-gather.3.cloned.1.call-start = ((), (), s32[]{:S(2)}) async-start(), calls=%async_computation.5 | async-start | bytes 4456448 | tf_op jit(solution)/shard_map/all_gather | solution.py:31
  8.4 121.0 %all-gather.5.cloned.1.call-start = ((), (), s32[]{:S(2)}) async-start(), calls=%async_computation.6 | async-start | bytes 8912896 | tf_op jit(solution)/shard_map/all_gather | solution.py:124
  10.5 71.0 %all-to-all-start = ((f32[16,512,2]{1,2,0:T(2,128)}), f32[16,512,2]{1,2,0:T(2,128)S(1)}, u32[]{:S(2)}, u32[]{:S(2)}) async-start(f32[16,512,2]{1,2,0:T(2,128)} %broadcast_in_dim.64), calls=%async_computation | async-start | bytes 131072 | tf_op jit(solution)/shard_map/all_to_all | solution.py:12
  73.6 7.9 %copy-start.2 = (f32[512,2]{0,1:T(2,128)S(1)}, f32[512,2]{0,1:T(2,128)}, u32[]{:S(2)}) copy-start(f32[512,2]{0,1:T(2,128)} %param.20) | copy-start | bytes 12292
  81.5 47.9 %copy-start.3 = (bf16[32,2048]{1,0:T(8,128)(2,1)S(1)}, bf16[32,2048]{1,0:T(8,128)(2,1)}, u32[]{:S(2)}) copy-start(bf16[32,2048]{1,0:T(8,128)(2,1)} %param.16) | copy-start | bytes 393220
  99.1 17.7 %all-to-all-start.1 = ((bf16[16,32,128]{2,1,0:T(8,128)(2,1)}), bf16[16,32,128]{2,1,0:T(8,128)(2,1)S(1)}, u32[]{:S(2)}, u32[]{:S(2)}) async-start(bf16[16,32,128]{2,1,0:T(8,128)(2,1)} %all_to_all.24), calls=%async_computation.1 | async-start | bytes 262144 | tf_op jit(solution)/shard_map/all_to_all | solution.py:121
  106.2 223.1 %reduce-scatter.2.cloned.1.call-start = ((), (), s32[]{:S(2)}) async-start(), calls=%async_computation.7 | async-start | bytes 6684672 | tf_op jit(solution)/shard_map/reduce_scatter | solution.py:165
  106.4 28.0 %copy-start.4 = (f32[2048]{0:T(1024)S(1)}, f32[2048]{0:T(1024)}, u32[]{:S(2)}) copy-start(f32[2048]{0:T(1024)} %param.22) | copy-start | bytes 24580
  180.3 8.4 %collective-permute-start = (bf16[96,2048]{1,0:T(8,128)(2,1)S(1)}, bf16[96,2048]{1,0:T(8,128)(2,1)S(1)}, u32[]{:S(2)}, u32[]{:S(2)}) collective-permute-start(bf16[96,2048]{1,0:T(8,128)(2,1)S(1)} %reshape.146), channel_id=1, source_target_pairs={{0,1},{1,2},{2,3},{3,4},{4,5},{5,6},{6,7},{7,8},{8,9},{9,10},{10,1... | collective-permute-start | bytes 1179656 | tf_op jit(solution)/shard_map/ppermute | solution.py:154
  180.3 8.4 %collective-permute-start.1 = (bf16[96,2048]{1,0:T(8,128)(2,1)S(1)}, bf16[96,2048]{1,0:T(8,128)(2,1)S(1)}, u32[]{:S(2)}, u32[]{:S(2)}) collective-permute-start(bf16[96,2048]{1,0:T(8,128)(2,1)S(1)} %reshape.146), channel_id=1, source_target_pairs={{0,15},{1,0},{2,1},{3,2},{4,3},{5,4},{6,5},{7,6},{8,7},{9,8},{10,9... | collective-permute-start | bytes 1179656 | tf_op jit(solution)/shard_map/ppermute | solution.py:157
  188.7 8.4 %collective-permute-start.2 = (bf16[96,2048]{1,0:T(8,128)(2,1)S(1)}, bf16[96,2048]{1,0:T(8,128)(2,1)S(1)}, u32[]{:S(2)}, u32[]{:S(2)}) collective-permute-start(bf16[96,2048]{1,0:T(8,128)(2,1)S(1)} %collective-permute-done), channel_id=1, source_target_pairs={{0,1},{1,2},{2,3},{3,4},{4,5},{5,6},{6,7},{7,8},{8,9},{9,10},{10,1... | collective-permute-start | bytes 1179656 | tf_op jit(solution)/shard_map/ppermute | solution.py:154
  188.7 8.4 %collective-permute-start.3 = (bf16[96,2048]{1,0:T(8,128)(2,1)S(1)}, bf16[96,2048]{1,0:T(8,128)(2,1)S(1)}, u32[]{:S(2)}, u32[]{:S(2)}) collective-permute-start(bf16[96,2048]{1,0:T(8,128)(2,1)S(1)} %collective-permute-done.1), channel_id=1, source_target_pairs={{0,15},{1,0},{2,1},{3,2},{4,3},{5,4},{6,5},{7,6},{8,7},{9,8},{10,9... | collective-permute-start | bytes 1179656 | tf_op jit(solution)/shard_map/ppermute | solution.py:157
  197.1 8.4 %collective-permute-start.4 = (bf16[96,2048]{1,0:T(8,128)(2,1)S(1)}, bf16[96,2048]{1,0:T(8,128)(2,1)S(1)}, u32[]{:S(2)}, u32[]{:S(2)}) collective-permute-start(bf16[96,2048]{1,0:T(8,128)(2,1)S(1)} %collective-permute-done.2), channel_id=1, source_target_pairs={{0,1},{1,2},{2,3},{3,4},{4,5},{5,6},{6,7},{7,8},{8,9},{9,10},{10,1... | collective-permute-start | bytes 1179656 | tf_op jit(solution)/shard_map/ppermute | solution.py:154
  197.1 8.4 %collective-permute-start.5 = (bf16[96,2048]{1,0:T(8,128)(2,1)S(1)}, bf16[96,2048]{1,0:T(8,128)(2,1)S(1)}, u32[]{:S(2)}, u32[]{:S(2)}) collective-permute-start(bf16[96,2048]{1,0:T(8,128)(2,1)S(1)} %collective-permute-done.3), channel_id=1, source_target_pairs={{0,15},{1,0},{2,1},{3,2},{4,3},{5,4},{6,5},{7,6},{8,7},{9,8},{10,9... | collective-permute-start | bytes 1179656 | tf_op jit(solution)/shard_map/ppermute | solution.py:157
  200.2 50.1 %copy-start.7 = (bf16[1,2048,448]{1,2,0:T(8,128)(2,1)S(1)}, bf16[1,2048,448]{1,2,0:T(8,128)(2,1)}, u32[]{:S(2)}) copy-start(bf16[1,2048,448]{1,2,0:T(8,128)(2,1)} %param.23) | copy-start | bytes 5505028
  205.5 8.4 %collective-permute-start.6 = (bf16[96,2048]{1,0:T(8,128)(2,1)S(1)}, bf16[96,2048]{1,0:T(8,128)(2,1)S(1)}, u32[]{:S(2)}, u32[]{:S(2)}) collective-permute-start(bf16[96,2048]{1,0:T(8,128)(2,1)S(1)} %collective-permute-done.4), channel_id=1, source_target_pairs={{0,1},{1,2},{2,3},{3,4},{4,5},{5,6},{6,7},{7,8},{8,9},{9,10},{10,1... | collective-permute-start | bytes 1179656 | tf_op jit(solution)/shard_map/ppermute | solution.py:154
  205.5 8.4 %collective-permute-start.7 = (bf16[96,2048]{1,0:T(8,128)(2,1)S(1)}, bf16[96,2048]{1,0:T(8,128)(2,1)S(1)}, u32[]{:S(2)}, u32[]{:S(2)}) collective-permute-start(bf16[96,2048]{1,0:T(8,128)(2,1)S(1)} %collective-permute-done.5), channel_id=1, source_target_pairs={{0,15},{1,0},{2,1},{3,2},{4,3},{5,4},{6,5},{7,6},{8,7},{9,8},{10,9... | collective-permute-start | bytes 1179656 | tf_op jit(solution)/shard_map/ppermute | solution.py:157
  213.9 8.4 %collective-permute-start.8 = (bf16[96,2048]{1,0:T(8,128)(2,1)S(1)}, bf16[96,2048]{1,0:T(8,128)(2,1)S(1)}, u32[]{:S(2)}, u32[]{:S(2)}) collective-permute-start(bf16[96,2048]{1,0:T(8,128)(2,1)S(1)} %collective-permute-done.6), channel_id=1, source_target_pairs={{0,1},{1,2},{2,3},{3,4},{4,5},{5,6},{6,7},{7,8},{8,9},{9,10},{10,1... | collective-permute-start | bytes 1179656 | tf_op jit(solution)/shard_map/ppermute | solution.py:154
  213.9 8.4 %collective-permute-start.9 = (bf16[96,2048]{1,0:T(8,128)(2,1)S(1)}, bf16[96,2048]{1,0:T(8,128)(2,1)S(1)}, u32[]{:S(2)}, u32[]{:S(2)}) collective-permute-start(bf16[96,2048]{1,0:T(8,128)(2,1)S(1)} %collective-permute-done.7), channel_id=1, source_target_pairs={{0,15},{1,0},{2,1},{3,2},{4,3},{5,4},{6,5},{7,6},{8,7},{9,8},{10,9... | collective-permute-start | bytes 1179656 | tf_op jit(solution)/shard_map/ppermute | solution.py:157
  222.4 8.4 %collective-permute-start.10 = (bf16[96,2048]{1,0:T(8,128)(2,1)S(1)}, bf16[96,2048]{1,0:T(8,128)(2,1)S(1)}, u32[]{:S(2)}, u32[]{:S(2)}) collective-permute-start(bf16[96,2048]{1,0:T(8,128)(2,1)S(1)} %collective-permute-done.8), channel_id=1, source_target_pairs={{0,1},{1,2},{2,3},{3,4},{4,5},{5,6},{6,7},{7,8},{8,9},{9,10},{10,1... | collective-permute-start | bytes 1179656 | tf_op jit(solution)/shard_map/ppermute | solution.py:154
  222.4 8.4 %collective-permute-start.11 = (bf16[96,2048]{1,0:T(8,128)(2,1)S(1)}, bf16[96,2048]{1,0:T(8,128)(2,1)S(1)}, u32[]{:S(2)}, u32[]{:S(2)}) collective-permute-start(bf16[96,2048]{1,0:T(8,128)(2,1)S(1)} %collective-permute-done.9), channel_id=1, source_target_pairs={{0,15},{1,0},{2,1},{3,2},{4,3},{5,4},{6,5},{7,6},{8,7},{9,8},{10,9... | collective-permute-start | bytes 1179656 | tf_op jit(solution)/shard_map/ppermute | solution.py:157
  230.8 8.4 %collective-permute-start.12 = (bf16[96,2048]{1,0:T(8,128)(2,1)S(1)}, bf16[96,2048]{1,0:T(8,128)(2,1)S(1)}, u32[]{:S(2)}, u32[]{:S(2)}) collective-permute-start(bf16[96,2048]{1,0:T(8,128)(2,1)S(1)} %collective-permute-done.10), channel_id=1, source_target_pairs={{0,1},{1,2},{2,3},{3,4},{4,5},{5,6},{6,7},{7,8},{8,9},{9,10},{10,1... | collective-permute-start | bytes 1179656 | tf_op jit(solution)/shard_map/ppermute | solution.py:154
  230.8 8.5 %collective-permute-start.13 = (bf16[96,2048]{1,0:T(8,128)(2,1)S(1)}, bf16[96,2048]{1,0:T(8,128)(2,1)S(1)}, u32[]{:S(2)}, u32[]{:S(2)}) collective-permute-start(bf16[96,2048]{1,0:T(8,128)(2,1)S(1)} %collective-permute-done.11), channel_id=1, source_target_pairs={{0,15},{1,0},{2,1},{3,2},{4,3},{5,4},{6,5},{7,6},{8,7},{9,8},{10,9... | collective-permute-start | bytes 1179656 | tf_op jit(solution)/shard_map/ppermute | solution.py:157
  239.2 8.4 %collective-permute-start.14 = (bf16[96,2048]{1,0:T(8,128)(2,1)S(1)}, bf16[96,2048]{1,0:T(8,128)(2,1)S(1)}, u32[]{:S(2)}, u32[]{:S(2)}) collective-permute-start(bf16[96,2048]{1,0:T(8,128)(2,1)S(1)} %collective-permute-done.12), channel_id=1, source_target_pairs={{0,1},{1,2},{2,3},{3,4},{4,5},{5,6},{6,7},{7,8},{8,9},{9,10},{10,1... | collective-permute-start | bytes 1179656 | tf_op jit(solution)/shard_map/ppermute | solution.py:154
  247.6 2.6 copy-start.1
  268.0 70.5 %copy-start.5 = (s32[32,2]{0,1:T(2,128)S(1)}, s32[32,2]{0,1:T(2,128)}, u32[]{:S(2)}) copy-start(s32[32,2]{0,1:T(2,128)} %param.26) | copy-start | bytes 772
  268.0 70.7 %copy-start.6 = (f32[32,2]{0,1:T(2,128)S(1)}, f32[32,2]{0,1:T(2,128)}, u32[]{:S(2)}) copy-start(f32[32,2]{0,1:T(2,128)} %param.27) | copy-start | bytes 772
  331.2 16.0 %all-to-all-start.3 = ((bf16[16,6,2048]{2,1,0:T(8,128)(2,1)}), bf16[16,6,2048]{2,1,0:T(8,128)(2,1)S(1)}, u32[]{:S(2)}, u32[]{:S(2)}) async-start(bf16[16,6,2048]{2,1,0:T(8,128)(2,1)} %reshape.147), calls=%async_computation.4 | async-start | bytes 1048576 | tf_op jit(solution)/shard_map/all_to_all | solution.py:172
Sparse Core Ops, SparseCore 0:
  9.8 59.3 all-gather.2
  71.0 58.3 all-gather.4
  268.2 61.0 reduce-scatter.1
